TPU v7x, 32 devices: a whole 2x2x4 slice. The times are simulated.
32 devices in a mesh: sp: 16 (over z, y, x), tp: 2 (over core).
Axes of the slice: x: 2, y: 2, z: 4, core: 2. Of those that a mesh axis runs over, the one named last changes fastest.
Arguments:
- residual: bfloat16 [4096, 2048], P('sp'), may hold values from -6 to 6
- queries: bfloat16 [4096, 1024], P('sp', 'tp'), may hold values from -6 to 6
- forget_gate_logits: bfloat16 [4096, 1024], P('sp', 'tp'), may hold values from -5 to 5
- projected_values: bfloat16 [4096, 1024], P('sp', 'tp'), may hold values from -6 to 6
- output_gate_logits: bfloat16 [4096, 1024], P('sp', 'tp'), may hold values from -6 to 6
- lower_bound_margin: float32 [1024], P('tp'), may hold values from 0.00024414062 to 0.08
- extra_forget_logs: float32 [4096, 1024], P('sp', 'tp'), may hold values from -0.7 to 0
- per_head_norm_gain: float32 [128], replicated, may hold values from 0.1 to 1.9
- output_weight: bfloat16 [1024, 2048], P('tp'), may hold values from -0.1875 to 0.1875
- feedforward_norm_gain: float32 [2048], replicated, may hold values from 0.1 to 1.9
- gate_weight: bfloat16 [2048, 5632], P('sp', 'tp'), may hold values from -0.125 to 0.125
- up_weight: bfloat16 [2048, 5632], P('sp', 'tp'), may hold values from -0.125 to 0.125
- down_weight: bfloat16 [5632, 2048], P('tp', 'sp'), may hold values from -0.078125 to 0.078125
Outputs:
- layer_out: bfloat16 [4096, 2048], P('sp')
All inputs are finite; a program needn't handle non-finite values.
Results may differ from a plain program's by a relative error of at most 0.015.
Values may be sent and summed in bfloat16 or wider, within the bound.
A program may use at most 128 MiB of HBM per device.

v0:
```python
import jax
import jax.numpy as jnp
from jax import lax
from jax.sharding import PartitionSpec as P

HD = 128
BLOCK = 64
eps = 1e-06
top_precision = lax.Precision.HIGHEST


def carried_in_2(value, axis, join, neutral):
    place = lax.axis_index(axis)
    gathered = jax.tree.map(
        lambda a, kind: lax.all_gather(a.astype(kind), axis), value, (jnp.bfloat16, jnp.bfloat16)
    )
    state = jax.tree.map(lambda a, e: jnp.zeros_like(a) + jnp.asarray(e, a.dtype), value, neutral)

    def one(turn, state):
        return join(
            state,
            jax.tree.map(
                lambda a, own: lax.dynamic_index_in_dim(a, turn, 0, False).astype(own.dtype),
                gathered,
                value,
            ),
        )

    return lax.fori_loop(0, place, one, state)


def block_update(carried_in, inputs):
    recurrent_state, offset = carried_in
    queries, state_increment, value_rows, retain_log_factor = inputs
    running_state = jnp.cumsum(retain_log_factor, axis=1)
    causal = jnp.tril(
        jnp.ones((retain_log_factor.shape[1], retain_log_factor.shape[1]), dtype=bool)
    )
    carried_over_state = jnp.einsum(
        "uqw,uwa->uqa", queries * jnp.exp(running_state), recurrent_state, precision=top_precision
    )
    spread = running_state[:, :, None, :] - running_state[:, None, :, :]
    weights = jnp.exp(jnp.where(causal[None, :, :, None], spread, -jnp.inf))
    scores = jnp.einsum(
        "htk,htsk,hsk->hts", queries, weights, state_increment, precision=top_precision
    )
    output_rows = carried_over_state + jnp.einsum(
        "hts,hsv->htv", scores, value_rows, precision=top_precision
    )
    final_state = running_state[:, -1:, :]
    updated_state = jnp.exp(final_state[:, 0, :])[:, :, None] * recurrent_state + jnp.einsum(
        "erb,erc->ebc",
        state_increment * jnp.exp(final_state - running_state),
        value_rows,
        precision=top_precision,
    )
    rescaled_state = queries * jnp.exp(running_state + offset[:, None, :])
    return ((updated_state, offset + final_state[:, 0, :]), (output_rows, rescaled_state))


def join_states(earlier, later):
    earlier_sum, earlier_memory = earlier
    later_sum, later_memory = later
    return (earlier_sum + later_sum, jnp.exp(later_sum)[:, :, None] * earlier_memory + later_memory)


def local(
    residual,
    queries,
    forget_gate_logits,
    projected_values,
    output_gate_logits,
    lower_bound_margin,
    extra_forget_logs,
    per_head_norm_gain,
    output_weight,
    feedforward_norm_gain,
    gate_weight,
    up_weight,
    down_weight,
):
    length = queries.shape[0]
    head_count = queries.shape[1] // HD
    state_increment = lower_bound_margin * jax.nn.sigmoid(-forget_gate_logits.astype(jnp.float32))
    retain_log_factor = jnp.log1p(-state_increment) + extra_forget_logs

    def to_blocks(source):
        return source.reshape(length // BLOCK, BLOCK, head_count, HD).transpose(0, 2, 1, 3)

    initial = (
        jnp.zeros((head_count, HD, HD), jnp.float32),
        jnp.zeros((head_count, HD), jnp.float32),
    )
    block_inputs = (
        to_blocks(queries.astype(jnp.float32)),
        to_blocks(state_increment),
        to_blocks(projected_values.astype(jnp.float32)),
        to_blocks(retain_log_factor),
    )
    (recurrent_state, decay_sum), (output_rows, rescaled_state) = lax.scan(
        block_update, initial, block_inputs
    )
    identity = (jnp.zeros_like(decay_sum), jnp.zeros_like(recurrent_state))
    incoming_state = carried_in_2((decay_sum, recurrent_state), "sp", join_states, identity)[1]
    output_rows = output_rows + jnp.einsum(
        "sjey,jyx->sjex", rescaled_state, incoming_state, precision=top_precision
    )
    mixed = output_rows.transpose(0, 2, 1, 3).reshape(length, head_count, HD)
    normed_heads = (
        mixed
        * lax.rsqrt(jnp.mean(mixed * mixed, axis=-1, keepdims=True) + eps)
        * per_head_norm_gain
    )
    gating = jax.nn.silu(output_gate_logits.astype(jnp.float32)).reshape(length, head_count, HD)
    gated = (normed_heads * gating).reshape(length, head_count * HD).astype(jnp.bfloat16)
    row_count = residual.shape[0] // lax.axis_size("tp")
    own_rows = lax.dynamic_slice_in_dim(residual, lax.axis_index("tp") * row_count, row_count, 0)
    rows_here = gated
    projected = lax.psum_scatter(
        jnp.dot(rows_here, output_weight, preferred_element_type=jnp.float32).astype(jnp.bfloat16),
        "tp",
        scatter_dimension=0,
        tiled=True,
    ).astype(jnp.float32)
    after_mixer = (own_rows.astype(jnp.float32) + projected).astype(jnp.bfloat16)
    widened = after_mixer.astype(jnp.float32)
    normed = (
        widened
        * lax.rsqrt(jnp.mean(widened * widened, axis=-1, keepdims=True) + eps)
        * feedforward_norm_gain
    ).astype(jnp.bfloat16)
    gate_full, up_full = (
        lax.all_gather(gate_weight, "sp", axis=0, tiled=True),
        lax.all_gather(up_weight, "sp", axis=0, tiled=True),
    )
    down_full = lax.all_gather(down_weight, "sp", axis=1, tiled=True)
    row_piece = lax.all_gather(normed, "tp", axis=0, tiled=True)
    gate_part = jnp.dot(row_piece, gate_full, preferred_element_type=jnp.float32)
    up_part = jnp.dot(row_piece, up_full, preferred_element_type=jnp.float32)
    hidden = (jax.nn.silu(gate_part) * up_part).astype(jnp.bfloat16)
    rows_here = hidden
    ffn_sum = lax.psum_scatter(
        jnp.dot(rows_here, down_full, preferred_element_type=jnp.float32).astype(jnp.bfloat16),
        "tp",
        scatter_dimension=0,
        tiled=True,
    ).astype(jnp.float32)
    finished = (after_mixer.astype(jnp.float32) + 0.5 * ffn_sum).astype(jnp.bfloat16)
    return lax.all_gather(finished, "tp", axis=0, tiled=True)


def solution(mesh):
    return jax.shard_map(
        local,
        mesh=mesh,
        in_specs=(
            P("sp", None),
            P("sp", "tp"),
            P("sp", "tp"),
            P("sp", "tp"),
            P("sp", "tp"),
            P("tp"),
            P("sp", "tp"),
            P(),
            P("tp", None),
            P(),
            P("sp", "tp"),
            P("sp", "tp"),
            P("tp", "sp"),
        ),
        out_specs=P("sp", None),
        check_vma=False,
    )
```

profile of v0, /device:TPU:0, one launch (start us, length us, event | category | flops | bytes accessed | tf_op | source)
XLA Modules:
  0.0 711.4 jit_solution(5645837955671285264)
XLA Ops:
  6.5 2.4 divide_multiply_fusion
  8.9 1.2 reshape.85
  11.1 1.9 reshape.91
  13.0 1.9 reshape.92
  15.0 75.4 %while.30 = (s32[]{:T(128)}, f32[4,128,128]{2,1,0:T(8,128)S(1)}, f32[4,128]{1,0:T(4,128)S(1)}, f32[4,4,64,128]{3,2,0,1:T(8,128)}, f32[4,4,64,128]{3,2,0,1:T(8,12...) while((s32[]{:T(128)}, f32[4,128,128]{2,1,0:T(8,128)S(1)}, ...), condition=%wide.region_2.3_spmd.clone, body=%wide.region_0.2_spmd.clone.sunk | while | flops 159814656 | bytes 5010573 | solution.py:100
  16.1 1.0 constant_dynamic-slice_fusion.7
  17.1 14.1 %fusion.72 = f32[4,64,1,64]{3,2,1,0:T(1,128)S(1)} fusion(f32[4,64,128,1]{2,3,1,0:T(1,128)S(1)} %bitcast.133, f32[4,64,128]{2,1,0:T(8,128)S(1)} %bitcast.134, f32[4,64,128]{2,1,0:T(8,128)S(1)} %reduce_window_sum.16, pred[64,64]{1,0:T(8,128)(4,1)S(1)} %iota_compare_fusion.2), kind=kOutput, calls=%fused_computation.2.clone.1 | convolution fusion | flops 31457280 | bytes 462848 | tf_op jit(solution)/shard_map/while/body/eval_jaxpr/htk,htsk,hsk->hts/dot_general | solution.py:44
  31.4 1.0 fusion.74
  34.9 1.0 constant_dynamic-slice_fusion.7
  35.9 14.1 %fusion.72 = f32[4,64,1,64]{3,2,1,0:T(1,128)S(1)} fusion(f32[4,64,128,1]{2,3,1,0:T(1,128)S(1)} %bitcast.133, f32[4,64,128]{2,1,0:T(8,128)S(1)} %bitcast.134, f32[4,64,128]{2,1,0:T(8,128)S(1)} %reduce_window_sum.16, pred[64,64]{1,0:T(8,128)(4,1)S(1)} %iota_compare_fusion.2), kind=kOutput, calls=%fused_computation.2.clone.1 | convolution fusion | flops 31457280 | bytes 462848 | tf_op jit(solution)/shard_map/while/body/eval_jaxpr/htk,htsk,hsk->hts/dot_general | solution.py:44
  50.3 1.0 fusion.74
  54.8 14.1 %fusion.72 = f32[4,64,1,64]{3,2,1,0:T(1,128)S(1)} fusion(f32[4,64,128,1]{2,3,1,0:T(1,128)S(1)} %bitcast.133, f32[4,64,128]{2,1,0:T(8,128)S(1)} %bitcast.134, f32[4,64,128]{2,1,0:T(8,128)S(1)} %reduce_window_sum.16, pred[64,64]{1,0:T(8,128)(4,1)S(1)} %iota_compare_fusion.2), kind=kOutput, calls=%fused_computation.2.clone.1 | convolution fusion | flops 31457280 | bytes 462848 | tf_op jit(solution)/shard_map/while/body/eval_jaxpr/htk,htsk,hsk->hts/dot_general | solution.py:44
  69.1 1.0 fusion.74
  72.6 1.0 constant_dynamic-slice_fusion.7
  73.6 14.1 %fusion.72 = f32[4,64,1,64]{3,2,1,0:T(1,128)S(1)} fusion(f32[4,64,128,1]{2,3,1,0:T(1,128)S(1)} %bitcast.133, f32[4,64,128]{2,1,0:T(8,128)S(1)} %bitcast.134, f32[4,64,128]{2,1,0:T(8,128)S(1)} %reduce_window_sum.16, pred[64,64]{1,0:T(8,128)(4,1)S(1)} %iota_compare_fusion.2), kind=kOutput, calls=%fused_computation.2.clone.1 | convolution fusion | flops 31457280 | bytes 462848 | tf_op jit(solution)/shard_map/while/body/eval_jaxpr/htk,htsk,hsk->hts/dot_general | solution.py:44
  88.0 1.0 fusion.74
  91.1 42.6 %all-gather.2 = bf16[16,4,128]{2,1,0:T(4,128)(2,1)S(1)} all-gather(bf16[1,4,128]{2,1,0:T(4,128)(2,1)S(1)} %convert_bitcast_fusion), channel_id=2, replica_groups=mesh['sp'=16,'tp'=2] {'sp'}, dimensions={0}, use_global_device_ids=true | all-gather | bytes 17408 | tf_op jit(solution)/shard_map/all_gather | solution.py:15
  133.7 20.7 %all-gather.20.cloned.1.call-done = bf16[64,128,128]{2,1,0:T(8,128)(2,1)} async-done(((bf16[4,128,128]{2,1,0:T(8,128)(2,1)}), bf16[64,128,128]{2,1,0:T(8,128)(2,1)}) %all-gather.20.cloned.1.call-update) | async-done | bytes 2097168 | tf_op jit(solution)/shard_map/all_gather | solution.py:15
  154.4 1.8 multiply_reduce_fusion
  157.0 2.7 convolution_convert_fusion.1
  159.8 24.2 %reduce-scatter.3.cloned.1.call-done = bf16[128,2048]{1,0:T(8,128)(2,1)} async-done(((bf16[256,2048]{1,0:T(8,128)(2,1)}), bf16[128,2048]{1,0:T(8,128)(2,1)}) %reduce-scatter.3.cloned.1.call-update) | async-done | bytes 524304 | tf_op jit(solution)/shard_map/reduce_scatter | solution.py:119
  184.0 1.5 fusion.30
  188.3 8.6 %all-gather.10.cloned.1.call-done = bf16[256,2048]{1,0:T(8,128)(2,1)} async-done(((bf16[128,2048]{1,0:T(8,128)(2,1)}), bf16[256,2048]{1,0:T(8,128)(2,1)}) %all-gather.10.cloned.1.call-update) | async-done | bytes 1048592 | tf_op jit(solution)/shard_map/all_gather | solution.py:137
  196.9 145.2 %all-gather.12.cloned.1.call-done = bf16[2048,2816]{1,0:T(8,128)(2,1)} async-done(((bf16[128,2816]{1,0:T(8,128)(2,1)}), bf16[2048,2816]{1,0:T(8,128)(2,1)}) %all-gather.12.cloned.1.call-update) | async-done | bytes 11534352 | tf_op jit(solution)/shard_map/all_gather | solution.py:133
  342.2 9.4 %fusion.47 = f32[256,2816]{1,0:T(8,128)} fusion(bf16[256,2048]{1,0:T(8,128)(2,1)} %all-gather.10.cloned.1.call-done, bf16[2048,2816]{1,0:T(8,128)(2,1)} %all-gather.12.cloned.1.call-done), kind=kOutput, calls=%fused_computation.80 | convolution fusion | flops 2952790016 | bytes 15466496 | tf_op jit(solution)/shard_map/dot_general | solution.py:138
  351.6 132.9 %all-gather.14.cloned.1.call-done = bf16[2048,2816]{1,0:T(8,128)(2,1)} async-done(((bf16[128,2816]{1,0:T(8,128)(2,1)}), bf16[2048,2816]{1,0:T(8,128)(2,1)}) %all-gather.14.cloned.1.call-update) | async-done | bytes 11534352 | tf_op jit(solution)/shard_map/all_gather | solution.py:134
  484.4 182.8 %all-gather.16.cloned.1.call-done = bf16[2816,2048]{1,0:T(8,128)(2,1)} async-done(((bf16[2816,128]{1,0:T(8,128)(2,1)}), bf16[2816,2048]{1,0:T(8,128)(2,1)}) %all-gather.16.cloned.1.call-update) | async-done | bytes 11534352 | tf_op jit(solution)/shard_map/all_gather | solution.py:136
  667.2 15.8 %convolution_convert_fusion = bf16[256,2048]{1,0:T(8,128)(2,1)} fusion(bf16[2816,2048]{1,0:T(8,128)(2,1)} %all-gather.16.cloned.1.call-done, bf16[256,2048]{1,0:T(8,128)(2,1)} %all-gather.10.cloned.1.call-done, bf16[2048,2816]{1,0:T(8,128)(2,1)} %all-gather.14.cloned.1.call-done, f32[256,2816]{1,0:T(8,128)} %fusion.47), kind=kOutput, calls=%fused_computation.45 | convolution fusion | flops 5910429696 | bytes 28049408 | tf_op jit(solution)/shard_map/dot_general | solution.py:143
  683.1 6.7 reduce-scatter.5.cloned.1.call-done
  689.8 2.0 fusion.33
  691.8 10.4 %all-gather.18.cloned.1.call-done = bf16[256,2048]{1,0:T(8,128)(2,1)} async-done(((bf16[128,2048]{1,0:T(8,128)(2,1)}), bf16[256,2048]{1,0:T(8,128)(2,1)}) %all-gather.18.cloned.1.call-update) | async-done | bytes 1048592 | tf_op jit(solution)/shard_map/all_gather | solution.py:149
  702.2 2.3 copy.110
  (85 shorter events, 17.3 us)
Async XLA Ops:
  6.5 150.5 %copy-start = (bf16[512,2048]{1,0:T(8,128)(2,1)S(1)}, bf16[512,2048]{1,0:T(8,128)(2,1)}, u32[]{:S(2)}) copy-start(bf16[512,2048]{1,0:T(8,128)(2,1)} %param.25) | copy-start | bytes 6291460
  6.5 147.8 %all-gather.20.cloned.1.call-start = ((), (), s32[]{:S(2)}) async-start(), calls=%async_computation.9 | async-start | bytes 2228224 | tf_op jit(solution)/shard_map/all_gather | solution.py:15
  15.0 118.7 %copy-start.3 = (f32[128]{0:T(128)S(1)}, f32[128]{0:T(128)}, u32[]{:S(2)}) copy-start(f32[128]{0:T(128)} %param.24) | copy-start | bytes 1540
  90.4 64.0 %copy-start.1 = (f32[4,4,64,128]{3,2,0,1:T(8,128)S(1)}, f32[4,4,64,128]{3,2,0,1:T(8,128)}, u32[]{:S(2)}) copy-start(f32[4,4,64,128]{3,2,0,1:T(8,128)} %get-tuple-element.99) | copy-start | bytes 1572868
  91.1 93.0 %reduce-scatter.3.cloned.1.call-start = ((), (), s32[]{:S(2)}) async-start(), calls=%async_computation.2 | async-start | bytes 1572864 | tf_op jit(solution)/shard_map/reduce_scatter | solution.py:119
  157.0 28.5 %copy-start.2 = (f32[2048]{0:T(1024)S(1)}, f32[2048]{0:T(1024)}, u32[]{:S(2)}) copy-start(f32[2048]{0:T(1024)} %param.26) | copy-start | bytes 24580
  159.8 37.2 %all-gather.10.cloned.1.call-start = ((), (), s32[]{:S(2)}) async-start(), calls=%async_computation.3 | async-start | bytes 1572864 | tf_op jit(solution)/shard_map/all_gather | solution.py:137
  186.5 155.6 %all-gather.12.cloned.1.call-start = ((), (), s32[]{:S(2)}) async-start(), calls=%async_computation.4 | async-start | bytes 12255232 | tf_op jit(solution)/shard_map/all_gather | solution.py:133
  187.1 297.3 %all-gather.14.cloned.1.call-start = ((), (), s32[]{:S(2)}) async-start(), calls=%async_computation.5 | async-start | bytes 12255232 | tf_op jit(solution)/shard_map/all_gather | solution.py:134
  187.7 479.5 %all-gather.16.cloned.1.call-start = ((), (), s32[]{:S(2)}) async-start(), calls=%async_computation.6 | async-start | bytes 12255232 | tf_op jit(solution)/shard_map/all_gather | solution.py:136
  188.3 501.5 %reduce-scatter.5.cloned.1.call-start = ((), (), s32[]{:S(2)}) async-start(), calls=%async_computation.7 | async-start | bytes 1572864 | tf_op jit(solution)/shard_map/reduce_scatter | solution.py:142
  683.1 19.1 %all-gather.18.cloned.1.call-start = ((), (), s32[]{:S(2)}) async-start(), calls=%async_computation.8 | async-start | bytes 1572864 | tf_op jit(solution)/shard_map/all_gather | solution.py:149
Sparse Core Ops, SparseCore 0:
  91.2 63.1 all-gather.19
  159.9 24.0 reduce-scatter.2
  186.7 10.2 all-gather.9
  199.6 142.5 all-gather.11
  344.8 139.5 all-gather.13
  487.0 180.2 all-gather.15
  683.2 6.5 reduce-scatter.4
  691.9 10.2 all-gather.17
where the time goes:
time: 712 us; the launch traced here: 711 us
  waiting for transfers between devices  533 us (75%)
  matrix products  93.7 us (13%)
  blocking collectives  42.6 us (6%)
  local copies, waits for them, and re-layouts  16.9 us (2%)
  between operations  13.6 us (2%)
  other arithmetic  10.9 us (2%)
    all_gather x1, waiting for transfers between devices, local(): down_full = lax.all_gather(down_weight, 'sp', axis=1, tiled=True)  183 us
    all_gather x1, waiting for transfers between devices, local(): lax.all_gather(gate_weight, 'sp', axis=0, tiled=True)  145 us
    all_gather x1, waiting for transfers between devices, local(): lax.all_gather(up_weight, 'sp', axis=0, tiled=True)  133 us
    dot_general x4, matrix products, block_update(): jnp.einsum('htk,htsk,hsk->hts', queries, weights, state_increment, precis...  56.2 us
    all_gather x1, blocking collectives, carried_in_2(): lax.all_gather(a.astype(kind), axis)  42.6 us
    reduce_scatter x1, waiting for transfers between devices, local(): lax.psum_scatter(jnp.dot(rows_here, output_weight, preferred_element_type...  24.2 us
    all_gather x1, waiting for transfers between devices, carried_in_2(): lax.all_gather(a.astype(kind), axis)  20.7 us
    dot_general x1, matrix products, local(): jnp.dot(rows_here, down_full, preferred_element_type=jnp.float32)  15.8 us
  transfers between devices with their start and end apart: 8, of which 8 were waited for; matrix products, arithmetic and copies ran while one was open for 1% of the time, Pallas kernels for 0%

commit v1 on v0

--- a/solution.py
+++ b/solution.py
@@ -133,7 +133,7 @@
         lax.all_gather(gate_weight, "sp", axis=0, tiled=True),
         lax.all_gather(up_weight, "sp", axis=0, tiled=True),
     )
-    down_full = lax.all_gather(down_weight, "sp", axis=1, tiled=True)
+    down_full = jnp.concatenate(lax.all_gather(down_weight, "sp"), axis=1)
     row_piece = lax.all_gather(normed, "tp", axis=0, tiled=True)
     gate_part = jnp.dot(row_piece, gate_full, preferred_element_type=jnp.float32)
     up_part = jnp.dot(row_piece, up_full, preferred_element_type=jnp.float32)

time: 712 us -> 671 us (0.942)
  waiting for transfers between devices: 533 us -> 476 us
  local copies, waits for them, and re-layouts: 16.9 us -> 32 us
    all_gather x1, waiting for transfers between devices: 183 us -> 142 us  [local(): down_full = jnp.concatenate(lax.all_gather(down_weight, 'sp'), axis=1)]
    reshape x0 -> x1, local copies, waits for them, and re-layouts: none -> 15.1 us  [local(): down_full = jnp.concatenate(lax.all_gather(down_weight, 'sp'), axis=1)]
    all_gather x1, waiting for transfers between devices: 8.62 us -> 0.01 us  [local(): row_piece = lax.all_gather(normed, 'tp', axis=0, tiled=True)]
  transfers between devices with their start and end apart: 8 -> 8, of which waited for: 8 -> 7; matrix products, arithmetic and copies ran while one was open for 1% -> 4% of each run, Pallas kernels for 0% -> 0%
where the time goes in v1:
time: 671 us; the launch traced here: 670 us
  waiting for transfers between devices  476 us (71%)
  matrix products  94 us (14%)
  blocking collectives  42.6 us (6%)
  local copies, waits for them, and re-layouts  32 us (5%)
  between operations  13.6 us (2%)
  other arithmetic  10.9 us (2%)
    all_gather x1, waiting for transfers between devices, local(): down_full = jnp.concatenate(lax.all_gather(down_weight, 'sp'), axis=1)  142 us
    all_gather x1, waiting for transfers between devices, local(): lax.all_gather(gate_weight, 'sp', axis=0, tiled=True)  139 us
    all_gather x1, waiting for transfers between devices, local(): lax.all_gather(up_weight, 'sp', axis=0, tiled=True)  133 us
    dot_general x4, matrix products, block_update(): jnp.einsum('htk,htsk,hsk->hts', queries, weights, state_increment, precis...  56.2 us
    all_gather x1, blocking collectives, carried_in_2(): lax.all_gather(a.astype(kind), axis)  42.6 us
    reduce_scatter x1, waiting for transfers between devices, local(): lax.psum_scatter(jnp.dot(rows_here, output_weight, preferred_element_type...  23.5 us
    all_gather x1, waiting for transfers between devices, carried_in_2(): lax.all_gather(a.astype(kind), axis)  20.7 us
    dot_general x1, matrix products, local(): jnp.dot(rows_here, down_full, preferred_element_type=jnp.float32)  15.9 us
  transfers between devices with their start and end apart: 8, of which 7 were waited for; matrix products, arithmetic and copies ran while one was open for 4% of the time, Pallas kernels for 0%

profile of v1, /device:TPU:0, one launch (start us, length us, event | category | flops | bytes accessed | tf_op | source)
XLA Modules:
  0.0 670.0 jit_solution(2691180283947078787)
XLA Ops:
  6.5 2.4 divide_multiply_fusion
  8.9 1.2 reshape.91
  11.1 1.9 reshape.99
  13.0 1.9 reshape.100
  15.0 75.4 %while.30 = (s32[]{:T(128)}, f32[4,128,128]{2,1,0:T(8,128)S(1)}, f32[4,128]{1,0:T(4,128)S(1)}, f32[4,4,64,128]{3,2,0,1:T(8,128)}, f32[4,4,64,128]{3,2,0,1:T(8,12...) while((s32[]{:T(128)}, f32[4,128,128]{2,1,0:T(8,128)S(1)}, ...), condition=%wide.region_2.3_spmd.clone, body=%wide.region_0.2_spmd.clone.sunk | while | flops 159814656 | bytes 5010573 | solution.py:100
  16.1 1.0 constant_dynamic-slice_fusion.7
  17.1 14.1 %fusion.72 = f32[4,64,1,64]{3,2,1,0:T(1,128)S(1)} fusion(f32[4,64,128,1]{2,3,1,0:T(1,128)S(1)} %bitcast.139, f32[4,64,128]{2,1,0:T(8,128)S(1)} %bitcast.140, f32[4,64,128]{2,1,0:T(8,128)S(1)} %reduce_window_sum.16, pred[64,64]{1,0:T(8,128)(4,1)S(1)} %iota_compare_fusion.2), kind=kOutput, calls=%fused_computation.2.clone.1 | convolution fusion | flops 31457280 | bytes 462848 | tf_op jit(solution)/shard_map/while/body/eval_jaxpr/htk,htsk,hsk->hts/dot_general | solution.py:44
  31.4 1.0 fusion.74
  34.9 1.0 constant_dynamic-slice_fusion.7
  35.9 14.1 %fusion.72 = f32[4,64,1,64]{3,2,1,0:T(1,128)S(1)} fusion(f32[4,64,128,1]{2,3,1,0:T(1,128)S(1)} %bitcast.139, f32[4,64,128]{2,1,0:T(8,128)S(1)} %bitcast.140, f32[4,64,128]{2,1,0:T(8,128)S(1)} %reduce_window_sum.16, pred[64,64]{1,0:T(8,128)(4,1)S(1)} %iota_compare_fusion.2), kind=kOutput, calls=%fused_computation.2.clone.1 | convolution fusion | flops 31457280 | bytes 462848 | tf_op jit(solution)/shard_map/while/body/eval_jaxpr/htk,htsk,hsk->hts/dot_general | solution.py:44
  50.3 1.0 fusion.74
  54.8 14.1 %fusion.72 = f32[4,64,1,64]{3,2,1,0:T(1,128)S(1)} fusion(f32[4,64,128,1]{2,3,1,0:T(1,128)S(1)} %bitcast.139, f32[4,64,128]{2,1,0:T(8,128)S(1)} %bitcast.140, f32[4,64,128]{2,1,0:T(8,128)S(1)} %reduce_window_sum.16, pred[64,64]{1,0:T(8,128)(4,1)S(1)} %iota_compare_fusion.2), kind=kOutput, calls=%fused_computation.2.clone.1 | convolution fusion | flops 31457280 | bytes 462848 | tf_op jit(solution)/shard_map/while/body/eval_jaxpr/htk,htsk,hsk->hts/dot_general | solution.py:44
  69.1 1.0 fusion.74
  72.6 1.0 constant_dynamic-slice_fusion.7
  73.6 14.1 %fusion.72 = f32[4,64,1,64]{3,2,1,0:T(1,128)S(1)} fusion(f32[4,64,128,1]{2,3,1,0:T(1,128)S(1)} %bitcast.139, f32[4,64,128]{2,1,0:T(8,128)S(1)} %bitcast.140, f32[4,64,128]{2,1,0:T(8,128)S(1)} %reduce_window_sum.16, pred[64,64]{1,0:T(8,128)(4,1)S(1)} %iota_compare_fusion.2), kind=kOutput, calls=%fused_computation.2.clone.1 | convolution fusion | flops 31457280 | bytes 462848 | tf_op jit(solution)/shard_map/while/body/eval_jaxpr/htk,htsk,hsk->hts/dot_general | solution.py:44
  88.0 1.0 fusion.74
  91.1 42.6 %all-gather.3 = bf16[16,4,128]{2,1,0:T(4,128)(2,1)S(1)} all-gather(bf16[1,4,128]{2,1,0:T(4,128)(2,1)S(1)} %convert_bitcast_fusion), channel_id=2, replica_groups=mesh['sp'=16,'tp'=2] {'sp'}, dimensions={0}, use_global_device_ids=true | all-gather | bytes 17408 | tf_op jit(solution)/shard_map/all_gather | solution.py:15
  133.7 20.7 %all-gather.19.cloned.1.call-done = bf16[64,128,128]{2,1,0:T(8,128)(2,1)} async-done(((bf16[4,128,128]{2,1,0:T(8,128)(2,1)}), bf16[64,128,128]{2,1,0:T(8,128)(2,1)}) %all-gather.19.cloned.1.call-update) | async-done | bytes 2097168 | tf_op jit(solution)/shard_map/all_gather | solution.py:15
  154.4 1.9 multiply_reduce_fusion
  157.2 2.7 convolution_convert_fusion.1
  160.7 23.5 %reduce-scatter.3.cloned.1.call-done = bf16[128,2048]{1,0:T(8,128)(2,1)} async-done(((bf16[256,2048]{1,0:T(8,128)(2,1)}), bf16[128,2048]{1,0:T(8,128)(2,1)}) %reduce-scatter.3.cloned.1.call-update) | async-done | bytes 524304 | tf_op jit(solution)/shard_map/reduce_scatter | solution.py:119
  184.2 1.5 fusion.30
  187.9 141.7 %all-gather.21.cloned.1.call-done = bf16[45056,128]{1,0:T(8,128)(2,1)} async-done(((bf16[2816,128]{1,0:T(8,128)(2,1)}), bf16[45056,128]{1,0:T(8,128)(2,1)}) %all-gather.21.cloned.1.call-update) | async-done | bytes 11534352 | tf_op jit(solution)/shard_map/all_gather | solution.py:136
  329.6 15.1 %copy.39 = bf16[2816,16,128]{0,2,1:T(8,128)(2,1)} copy(bf16[2816,16,128]{2,0,1:T(8,128)(2,1)} %bitcast.136) | data formatting | bytes 23068672 | tf_op jit(solution)/shard_map/reshape | solution.py:136
  344.7 138.7 %all-gather.13.cloned.1.call-done = bf16[2048,2816]{1,0:T(8,128)(2,1)} async-done(((bf16[128,2816]{1,0:T(8,128)(2,1)}), bf16[2048,2816]{1,0:T(8,128)(2,1)}) %all-gather.13.cloned.1.call-update) | async-done | bytes 11534352 | tf_op jit(solution)/shard_map/all_gather | solution.py:133
  483.5 9.4 %fusion.47 = f32[256,2816]{1,0:T(8,128)} fusion(bf16[256,2048]{1,0:T(8,128)(2,1)} %all-gather.11.cloned.1.call-done, bf16[2048,2816]{1,0:T(8,128)(2,1)} %all-gather.13.cloned.1.call-done), kind=kOutput, calls=%fused_computation.80 | convolution fusion | flops 2952790016 | bytes 15466496 | tf_op jit(solution)/shard_map/dot_general | solution.py:138
  492.9 132.8 %all-gather.15.cloned.1.call-done = bf16[2048,2816]{1,0:T(8,128)(2,1)} async-done(((bf16[128,2816]{1,0:T(8,128)(2,1)}), bf16[2048,2816]{1,0:T(8,128)(2,1)}) %all-gather.15.cloned.1.call-update) | async-done | bytes 11534352 | tf_op jit(solution)/shard_map/all_gather | solution.py:134
  625.7 15.9 %convolution_convert_fusion = bf16[256,2048]{1,0:T(8,128)(2,1)} fusion(bf16[2816,2048]{0,1:T(8,128)(2,1)} %bitcast.137, bf16[256,2048]{1,0:T(8,128)(2,1)} %all-gather.11.cloned.1.call-done, bf16[2048,2816]{1,0:T(8,128)(2,1)} %all-gather.15.cloned.1.call-done, f32[256,2816]{1,0:T(8,128)} %fusion.47), kind=kOutput, calls=%fused_computation.45 | convolution fusion | flops 5910429696 | bytes 28049408 | tf_op jit(solution)/shard_map/dot_general | solution.py:143
  641.8 6.7 reduce-scatter.5.cloned.1.call-done
  648.4 2.0 fusion.33
  650.5 10.4 %all-gather.17.cloned.1.call-done = bf16[256,2048]{1,0:T(8,128)(2,1)} async-done(((bf16[128,2048]{1,0:T(8,128)(2,1)}), bf16[256,2048]{1,0:T(8,128)(2,1)}) %all-gather.17.cloned.1.call-update) | async-done | bytes 1048592 | tf_op jit(solution)/shard_map/all_gather | solution.py:149
  660.9 2.3 copy.119
  (86 shorter events, 17.5 us)
Async XLA Ops:
  6.5 150.6 %copy-start = (bf16[512,2048]{1,0:T(8,128)(2,1)S(1)}, bf16[512,2048]{1,0:T(8,128)(2,1)}, u32[]{:S(2)}) copy-start(bf16[512,2048]{1,0:T(8,128)(2,1)} %param.25) | copy-start | bytes 6291460
  6.5 147.8 %all-gather.19.cloned.1.call-start = ((), (), s32[]{:S(2)}) async-start(), calls=%async_computation.8 | async-start | bytes 2228224 | tf_op jit(solution)/shard_map/all_gather | solution.py:15
  15.0 118.7 %copy-start.3 = (f32[128]{0:T(128)S(1)}, f32[128]{0:T(128)}, u32[]{:S(2)}) copy-start(f32[128]{0:T(128)} %param.24) | copy-start | bytes 1540
  91.0 94.6 %copy-start.2 = (f32[2048]{0:T(1024)S(1)}, f32[2048]{0:T(1024)}, u32[]{:S(2)}) copy-start(f32[2048]{0:T(1024)} %param.26) | copy-start | bytes 24580
  91.1 93.1 %reduce-scatter.3.cloned.1.call-start = ((), (), s32[]{:S(2)}) async-start(), calls=%async_computation.2 | async-start | bytes 1572864 | tf_op jit(solution)/shard_map/reduce_scatter | solution.py:119
  159.9 169.7 %all-gather.21.cloned.1.call-start = ((), (), s32[]{:S(2)}) async-start(), calls=%async_computation.9 | async-start | bytes 12255232 | tf_op jit(solution)/shard_map/all_gather | solution.py:136
  160.7 184.1 %all-gather.11.cloned.1.call-start = ((), (), s32[]{:S(2)}) async-start(), calls=%async_computation.3 | async-start | bytes 1572864 | tf_op jit(solution)/shard_map/all_gather | solution.py:137
  186.7 296.8 %all-gather.13.cloned.1.call-start = ((), (), s32[]{:S(2)}) async-start(), calls=%async_computation.4 | async-start | bytes 12255232 | tf_op jit(solution)/shard_map/all_gather | solution.py:133
  187.3 438.5 %all-gather.15.cloned.1.call-start = ((), (), s32[]{:S(2)}) async-start(), calls=%async_computation.5 | async-start | bytes 12255232 | tf_op jit(solution)/shard_map/all_gather | solution.py:134
  187.9 460.6 %reduce-scatter.5.cloned.1.call-start = ((), (), s32[]{:S(2)}) async-start(), calls=%async_computation.6 | async-start | bytes 1572864 | tf_op jit(solution)/shard_map/reduce_scatter | solution.py:142
  625.7 37.4 %copy-start.1 = (bf16[512,2048]{1,0:T(8,128)(2,1)S(1)}, bf16[512,2048]{1,0:T(8,128)(2,1)}, u32[]{:S(2)}) copy-start(bf16[512,2048]{1,0:T(8,128)(2,1)} %param.25) | copy-start | bytes 6291460
  641.7 19.1 %all-gather.17.cloned.1.call-start = ((), (), s32[]{:S(2)}) async-start(), calls=%async_computation.7 | async-start | bytes 1572864 | tf_op jit(solution)/shard_map/all_gather | solution.py:149
Sparse Core Ops, SparseCore 0:
  91.2 63.1 all-gather.18
  160.0 24.1 reduce-scatter.2
  187.0 142.6 all-gather.20
  331.0 7.1 all-gather.10
  340.9 142.5 all-gather.12
  486.1 139.5 all-gather.14
  641.8 6.5 reduce-scatter.4
  650.6 10.2 all-gather.16
